TPU v7x, 32 devices: a whole 2x2x4 slice. The times are simulated.
32 devices in a mesh: fs: 8 (over z, x), tp: 4 (over y, core).
Axes of the slice: x: 2, y: 2, z: 4, core: 2. Of those that a mesh axis runs over, the one named last changes fastest.
Arguments:
- prompt_rows: bfloat16 [512, 3072], P('tp'), may hold values from -6 to 6
- gate_first: float32 [3072, 8192], P('fs', 'tp'), may hold values from -0.109375 to 0.109375
- up_first: float32 [3072, 8192], P('fs', 'tp'), may hold values from -0.109375 to 0.109375
- down_first: float32 [8192, 3072], P('fs', 'tp'), may hold values from -0.0625 to 0.0625
- gate_second: float32 [3072, 8192], P('fs', 'tp'), may hold values from -0.109375 to 0.109375
- up_second: float32 [3072, 8192], P('fs', 'tp'), may hold values from -0.109375 to 0.109375
- down_second: float32 [8192, 3072], P('fs', 'tp'), may hold values from -0.0625 to 0.0625
- pre_gain_first: float32 [3072], replicated, may hold values from 0.1 to 1.9
- post_gain_first: float32 [3072], replicated, may hold values from 0.1 to 1.9
- pre_gain_second: float32 [3072], replicated, may hold values from 0.1 to 1.9
- post_gain_second: float32 [3072], replicated, may hold values from 0.1 to 1.9
Outputs:
- result_rows: bfloat16 [512, 3072], P('tp')
- gate_first_new: bfloat16 [3072, 8192], P(None, 'fs')
- up_first_new: bfloat16 [3072, 8192], P(None, 'fs')
- down_first_new: bfloat16 [8192, 3072], P('fs')
- gate_second_new: bfloat16 [3072, 8192], P(None, 'fs')
- up_second_new: bfloat16 [3072, 8192], P(None, 'fs')
- down_second_new: bfloat16 [8192, 3072], P('fs')
All inputs are finite; a program needn't handle non-finite values.
Results may differ from a plain program's by a relative error of at most 0.0071.
Values may be sent and summed in bfloat16 or wider, within the bound.
A program may use at most 192 MiB of HBM per device.

v0:
```python
import jax
import jax.numpy as jnp
from jax import lax
from jax.sharding import PartitionSpec as P

EPSILON = 1e-06


def half_step(rows, gate, up, down, post_gain):
    floats = rows.astype(jnp.float32)
    normed = (
        floats * lax.rsqrt(jnp.mean(floats * floats, axis=-1, keepdims=True) + EPSILON)
    ).astype(jnp.bfloat16)
    gate_pre = jnp.dot(normed, gate, preferred_element_type=jnp.float32)
    up_pre = jnp.dot(normed, up, preferred_element_type=jnp.float32)
    hidden = (jax.nn.silu(gate_pre) * up_pre).astype(jnp.bfloat16)
    partial_value = jnp.dot(hidden, down, preferred_element_type=jnp.float32)
    total = lax.psum(partial_value, "fs")
    scale = lax.rsqrt(jnp.mean(total * total, axis=-1, keepdims=True) + EPSILON)
    return (floats + 0.5 * total * scale * post_gain[None, :]).astype(jnp.bfloat16)


def per_device(
    prompt_rows,
    gate_first,
    up_first,
    down_first,
    gate_second,
    up_second,
    down_second,
    pre_gain_first,
    post_gain_first,
    pre_gain_second,
    post_gain_second,
):
    height = gate_first.shape[0]
    start = lax.axis_index("fs") * height
    gain_a = lax.dynamic_slice_in_dim(pre_gain_first, start, height, 0)[:, None]
    gain_b = lax.dynamic_slice_in_dim(pre_gain_second, start, height, 0)[:, None]
    wide = (
        lax.all_gather((gain_a * gate_first).astype(jnp.bfloat16), "tp", axis=1, tiled=True),
        lax.all_gather((gain_a * up_first).astype(jnp.bfloat16), "tp", axis=1, tiled=True),
        lax.all_gather(down_first.astype(jnp.bfloat16), "tp", axis=1, tiled=True),
        lax.all_gather((gain_b * gate_second).astype(jnp.bfloat16), "tp", axis=1, tiled=True),
        lax.all_gather((gain_b * up_second).astype(jnp.bfloat16), "tp", axis=1, tiled=True),
        lax.all_gather(down_second.astype(jnp.bfloat16), "tp", axis=1, tiled=True),
    )
    gate_a, up_a, gate_b, up_b = (
        lax.all_to_all(wide[0], "fs", split_axis=1, concat_axis=0, tiled=True),
        lax.all_to_all(wide[1], "fs", split_axis=1, concat_axis=0, tiled=True),
        lax.all_to_all(wide[3], "fs", split_axis=1, concat_axis=0, tiled=True),
        lax.all_to_all(wide[4], "fs", split_axis=1, concat_axis=0, tiled=True),
    )
    down_a = wide[2]
    down_b = wide[5]
    middle = half_step(prompt_rows, gate_a, up_a, down_a, post_gain_first)
    result = half_step(middle, gate_b, up_b, down_b, post_gain_second)
    return (result, gate_a, up_a, down_a, gate_b, up_b, down_b)


def solution(mesh):
    return jax.shard_map(
        per_device,
        mesh=mesh,
        in_specs=(
            P("tp", None),
            P("fs", "tp"),
            P("fs", "tp"),
            P("fs", "tp"),
            P("fs", "tp"),
            P("fs", "tp"),
            P("fs", "tp"),
            P(),
            P(),
            P(),
            P(),
        ),
        out_specs=(
            P("tp", None),
            P(None, "fs"),
            P(None, "fs"),
            P("fs", None),
            P(None, "fs"),
            P(None, "fs"),
            P("fs", None),
        ),
        check_vma=False,
    )
```

profile of v0, /device:TPU:0, one launch (start us, length us, event | category | flops | bytes accessed | tf_op | source)
XLA Modules:
  0.0 843.3 jit_solution(3647729259422297711)
XLA Ops:
  7.2 0.0 all-gather.7.cloned.1.call-start
  7.2 0.8 dynamic_slice.6
  8.0 5.5 multiply_convert_fusion.3
  13.5 0.0 all-gather.9.cloned.1.call-start
  13.6 0.7 all-gather.9.cloned.1.call-update
  14.3 48.5 %all-gather.7.cloned.1.call-done = bf16[384,8192]{1,0:T(8,128)(2,1)} async-done(((bf16[384,2048]{1,0:T(8,128)(2,1)}), bf16[384,8192]{1,0:T(8,128)(2,1)}) %all-gather.7.cloned.1.call-update) | async-done | bytes 6291472 | tf_op jit(solution)/shard_map/all_gather | solution.py:41
  62.7 6.5 copy.33
  69.2 5.8 all-to-all-start
  75.0 0.0 all-gather.13.cloned.1.call-start
  75.1 0.8 dynamic_slice.7
  75.8 4.5 multiply_convert_fusion.1
  80.4 30.9 %all-gather.9.cloned.1.call-done = bf16[384,8192]{1,0:T(8,128)(2,1)} async-done(((bf16[384,2048]{1,0:T(8,128)(2,1)}), bf16[384,8192]{1,0:T(8,128)(2,1)}) %all-gather.9.cloned.1.call-update) | async-done | bytes 6291472 | tf_op jit(solution)/shard_map/all_gather | solution.py:42
  111.3 6.5 copy.32
  117.8 95.9 %all-to-all-done = bf16[384,8,1024]{2,0,1:T(8,128)(2,1)} async-done(((bf16[384,8,1024]{2,0,1:T(8,128)(2,1)}), bf16[384,8,1024]{2,0,1:T(8,128)(2,1)}, u32[]{:S(2)}, u32[]{:S(2)}) %all-to-all-start) | async-done | bytes 6291488 | tf_op jit(solution)/shard_map/all_to_all | solution.py:49
  213.7 4.8 all-to-all-start.1
  218.4 0.0 all-gather.15.cloned.1.call-start
  218.5 0.5 all-gather.15.cloned.1.call-update
  219.0 6.5 copy.31
  225.5 130.6 %all-to-all-done.1 = bf16[384,8,1024]{2,0,1:T(8,128)(2,1)} async-done(((bf16[384,8,1024]{2,0,1:T(8,128)(2,1)}), bf16[384,8,1024]{2,0,1:T(8,128)(2,1)}, u32[]{:S(2)}, u32[]{:S(2)}) %all-to-all-start.1) | async-done | bytes 6291488 | tf_op jit(solution)/shard_map/all_to_all | solution.py:50
  356.1 4.8 all-to-all-start.2
  361.0 0.0 all-gather.11.cloned.1.call-start
  361.0 3.2 convert_element_type.47
  364.3 0.0 all-reduce.3.cloned.1.call-start
  364.4 0.2 fusion
  364.6 6.5 copy.30
  371.1 4.6 fusion.26
  375.7 35.5 %all-gather.11.cloned.1.call-done = bf16[1024,3072]{1,0:T(8,128)(2,1)} async-done(((bf16[1024,768]{1,0:T(8,128)(2,1)}), bf16[1024,3072]{1,0:T(8,128)(2,1)}) %all-gather.11.cloned.1.call-update) | async-done | bytes 6291472 | tf_op jit(solution)/shard_map/all_gather | solution.py:43
  411.2 7.7 fusion.9
  418.9 100.4 %all-to-all-done.2 = bf16[384,8,1024]{2,0,1:T(8,128)(2,1)} async-done(((bf16[384,8,1024]{2,0,1:T(8,128)(2,1)}), bf16[384,8,1024]{2,0,1:T(8,128)(2,1)}, u32[]{:S(2)}, u32[]{:S(2)}) %all-to-all-start.2) | async-done | bytes 6291488 | tf_op jit(solution)/shard_map/all_to_all | solution.py:51
  519.3 4.8 all-to-all-start.3
  524.1 0.0 all-gather.17.cloned.1.call-start
  524.2 3.3 convert_element_type.54
  527.4 0.2 all-reduce.5.cloned.1.call-start
  527.7 130.8 %all-reduce.3.cloned.1.call-done = f32[128,3072]{1,0:T(8,128)} async-done(((f32[128,3072]{1,0:T(8,128)}), f32[128,3072]{1,0:T(8,128)}) %all-reduce.3.cloned.1.call-update) | async-done | bytes 1572880 | tf_op jit(solution)/shard_map/psum | solution.py:18
  658.5 1.6 multiply_reduce_fusion.1
  660.1 1.9 fusion.3
  662.0 4.2 fusion.22
  666.3 38.0 %all-gather.17.cloned.1.call-done = bf16[1024,3072]{1,0:T(8,128)(2,1)} async-done(((bf16[1024,768]{1,0:T(8,128)(2,1)}), bf16[1024,3072]{1,0:T(8,128)(2,1)}) %all-gather.17.cloned.1.call-update) | async-done | bytes 6291472 | tf_op jit(solution)/shard_map/all_gather | solution.py:46
  704.2 7.7 fusion.8
  712.0 89.4 %all-reduce.5.cloned.1.call-done = f32[128,3072]{1,0:T(8,128)} async-done(((f32[128,3072]{1,0:T(8,128)}), f32[128,3072]{1,0:T(8,128)}) %all-reduce.5.cloned.1.call-update) | async-done | bytes 1572880 | tf_op jit(solution)/shard_map/psum | solution.py:18
  801.4 1.6 multiply_reduce_fusion
  803.0 2.6 fusion.5
  805.6 6.4 copy.42
  812.0 6.3 copy.43
  818.3 2.7 copy.44
  821.0 6.4 copy.45
  827.4 6.3 copy.46
  833.8 2.7 copy.47
  (31 shorter events, 0.2 us)
Async XLA Ops:
  7.2 55.6 %all-gather.7.cloned.1.call-start = ((), (), s32[]{:S(2)}) async-start(), calls=%async_computation.4 | async-start | bytes 7864320 | tf_op jit(solution)/shard_map/all_gather | solution.py:41
  13.5 97.8 %all-gather.9.cloned.1.call-start = ((), (), s32[]{:S(2)}) async-start(), calls=%async_computation.5 | async-start | bytes 7864320 | tf_op jit(solution)/shard_map/all_gather | solution.py:42
  69.2 6.6 copy-start.1
  69.2 144.4 %all-to-all-start = ((bf16[384,8,1024]{2,0,1:T(8,128)(2,1)}), bf16[384,8,1024]{2,0,1:T(8,128)(2,1)}, u32[]{:S(2)}, u32[]{:S(2)}) async-start(bf16[384,8,1024]{2,0,1:T(8,128)(2,1)} %bitcast.40), calls=%async_computation | async-start | bytes 12582912 | tf_op jit(solution)/shard_map/all_to_all | solution.py:49
  75.0 144.0 %all-gather.13.cloned.1.call-start = ((), (), s32[]{:S(2)}) async-start(), calls=%async_computation.8 | async-start | bytes 7864320 | tf_op jit(solution)/shard_map/all_gather | solution.py:44
  213.7 142.5 %all-to-all-start.1 = ((bf16[384,8,1024]{2,0,1:T(8,128)(2,1)}), bf16[384,8,1024]{2,0,1:T(8,128)(2,1)}, u32[]{:S(2)}, u32[]{:S(2)}) async-start(bf16[384,8,1024]{2,0,1:T(8,128)(2,1)} %bitcast.41), calls=%async_computation.1 | async-start | bytes 12582912 | tf_op jit(solution)/shard_map/all_to_all | solution.py:50
  218.4 146.2 %all-gather.15.cloned.1.call-start = ((), (), s32[]{:S(2)}) async-start(), calls=%async_computation.9 | async-start | bytes 7864320 | tf_op jit(solution)/shard_map/all_gather | solution.py:45
  356.1 163.1 %all-to-all-start.2 = ((bf16[384,8,1024]{2,0,1:T(8,128)(2,1)}), bf16[384,8,1024]{2,0,1:T(8,128)(2,1)}, u32[]{:S(2)}, u32[]{:S(2)}) async-start(bf16[384,8,1024]{2,0,1:T(8,128)(2,1)} %bitcast.39), calls=%async_computation.2 | async-start | bytes 12582912 | tf_op jit(solution)/shard_map/all_to_all | solution.py:51
  361.0 3.4 copy-start
  361.0 50.2 %all-gather.11.cloned.1.call-start = ((), (), s32[]{:S(2)}) async-start(), calls=%async_computation.6 | async-start | bytes 7864320 | tf_op jit(solution)/shard_map/all_gather | solution.py:43
  364.3 294.2 %all-reduce.3.cloned.1.call-start = ((), (), s32[]{:S(2)}) async-start(), calls=%async_computation.7 | async-start | bytes 3145728 | tf_op jit(solution)/shard_map/psum | solution.py:18
  519.3 185.0 %all-to-all-start.3 = ((bf16[384,8,1024]{2,0,1:T(8,128)(2,1)}), bf16[384,8,1024]{2,0,1:T(8,128)(2,1)}, u32[]{:S(2)}, u32[]{:S(2)}) async-start(bf16[384,8,1024]{2,0,1:T(8,128)(2,1)} %bitcast.38), calls=%async_computation.3 | async-start | bytes 12582912 | tf_op jit(solution)/shard_map/all_to_all | solution.py:52
  524.1 136.0 %copy-start.2 = (f32[3072]{0:T(1024)S(1)}, f32[3072]{0:T(1024)}, u32[]{:S(2)}) copy-start(f32[3072]{0:T(1024)} %param.19) | copy-start | bytes 36868
  524.1 180.1 %all-gather.17.cloned.1.call-start = ((), (), s32[]{:S(2)}) async-start(), calls=%async_computation.10 | async-start | bytes 7864320 | tf_op jit(solution)/shard_map/all_gather | solution.py:46
  527.4 273.9 %all-reduce.5.cloned.1.call-start = ((), (), s32[]{:S(2)}) async-start(), calls=%async_computation.11 | async-start | bytes 3145728 | tf_op jit(solution)/shard_map/psum | solution.py:18
  711.9 91.1 %copy-start.3 = (f32[3072]{0:T(1024)S(1)}, f32[3072]{0:T(1024)}, u32[]{:S(2)}) copy-start(f32[3072]{0:T(1024)} %param.21) | copy-start | bytes 36868
  805.6 12.7 %slice-start = ((s8[6291456]{0:T(1024)(128)(4,1)}), s8[4194304]{0:T(1024)(128)(4,1)S(1)}, s32[]{:S(2)}) async-start(s8[6291456]{0:T(1024)(128)(4,1)} %bitcast.34), calls=%async_computation.12 | async-start | bytes 8388608
  812.0 6.4 slice-start.1
  821.0 12.7 %slice-start.2 = ((s8[6291456]{0:T(1024)(128)(4,1)}), s8[4194304]{0:T(1024)(128)(4,1)S(1)}, s32[]{:S(2)}) async-start(s8[6291456]{0:T(1024)(128)(4,1)} %bitcast.36), calls=%async_computation.14 | async-start | bytes 8388608
  827.4 6.4 slice-start.3
Sparse Core Ops, SparseCore 0:
  13.6 49.0 all-gather.6
  64.9 46.3 all-gather.8
  113.4 46.3 all-gather.12
  221.1 46.7 all-gather.14
  364.4 46.6 all-gather.10
  419.0 239.4 all-reduce.2
  660.6 43.5 all-gather.16
  712.1 89.2 all-reduce.4
where the time goes:
time: 844 us; the launch traced here: 843 us
  waiting for transfers between devices  701 us (83%)
  local copies, waits for them, and re-layouts  58.5 us (7%)
  other arithmetic  24.5 us (3%)
  matrix products  24.2 us (3%)
  starting transfers between devices  20.7 us (2%)
  between operations  14.3 us (2%)
    psum x2, waiting for transfers between devices, half_step(): total = lax.psum(partial_value, 'fs')  220 us
    all_to_all x1, waiting for transfers between devices, per_device(): lax.all_to_all(wide[1], 'fs', split_axis=1, concat_axis=0, tiled=True)  131 us
    all_to_all x1, waiting for transfers between devices, per_device(): lax.all_to_all(wide[3], 'fs', split_axis=1, concat_axis=0, tiled=True)  100 us
    all_to_all x1, waiting for transfers between devices, per_device(): lax.all_to_all(wide[0], 'fs', split_axis=1, concat_axis=0, tiled=True)  95.9 us
    all_gather x1, waiting for transfers between devices, per_device(): lax.all_gather((gain_a * gate_first).astype(jnp.bfloat16), 'tp', axis=1,...  48.5 us
    all_gather x1, waiting for transfers between devices, per_device(): lax.all_gather(down_second.astype(jnp.bfloat16), 'tp', axis=1, tiled=True)  38 us
    all_gather x1, waiting for transfers between devices, per_device(): lax.all_gather(down_first.astype(jnp.bfloat16), 'tp', axis=1, tiled=True)  35.5 us
    unnamed x22, local copies, waits for them, and re-layouts  30.9 us
  transfers between devices with their start and end apart: 12, of which 9 were waited for; matrix products, arithmetic and copies ran while one was open for 7% of the time, Pallas kernels for 0%

commit v1 on v0

--- a/solution.py
+++ b/solution.py
@@ -33,12 +33,34 @@
     pre_gain_second,
     post_gain_second,
 ):
+
+    def arrange_thing_over_axis(matrix):
+        t_next = lax.axis_size("tp")
+        r_now, moved, mixed_arr = (t_next, lax.axis_index("tp"), matrix.shape[1])
+        buffers = tuple(((it, (it + 1) % r_now) for it in range(r_now)))
+        w1 = jnp.zeros((*matrix.shape[:1], r_now * mixed_arr, *matrix.shape[2:]), matrix.dtype)
+        rack = tuple(((it, (it - 1) % r_now) for it in range(r_now)))
+        w1 = lax.dynamic_update_slice_in_dim(w1, matrix, moved * mixed_arr, axis=1)
+        mid_arr = even = matrix
+        current_arr = r_now // 2
+        for ii in tuple(range(1, current_arr + 1)):
+            mid_arr = lax.ppermute(mid_arr, axis_name="tp", perm=buffers)
+            w1 = lax.dynamic_update_slice_in_dim(
+                w1, mid_arr, (moved - ii) % r_now * mixed_arr, axis=1
+            )
+            if ii < r_now - current_arr:
+                even = lax.ppermute(even, "tp", rack)
+                w1 = lax.dynamic_update_slice_in_dim(
+                    w1, even, (moved + ii) % r_now * mixed_arr, axis=1
+                )
+        return w1
+
     height = gate_first.shape[0]
     start = lax.axis_index("fs") * height
     gain_a = lax.dynamic_slice_in_dim(pre_gain_first, start, height, 0)[:, None]
     gain_b = lax.dynamic_slice_in_dim(pre_gain_second, start, height, 0)[:, None]
     wide = (
-        lax.all_gather((gain_a * gate_first).astype(jnp.bfloat16), "tp", axis=1, tiled=True),
+        arrange_thing_over_axis((gain_a * gate_first).astype(jnp.bfloat16)),
         lax.all_gather((gain_a * up_first).astype(jnp.bfloat16), "tp", axis=1, tiled=True),
         lax.all_gather(down_first.astype(jnp.bfloat16), "tp", axis=1, tiled=True),
         lax.all_gather((gain_b * gate_second).astype(jnp.bfloat16), "tp", axis=1, tiled=True),

time: 844 us -> 878 us (1.040)
  waiting for transfers between devices: 701 us -> 719 us
  starting transfers between devices: 20.7 us -> 30.7 us
    ppermute x0 -> x3, waiting for transfers between devices: none -> 75 us  [the longest x2 75 us: arrange_thing_over_axis(): mid_arr = lax.ppermute(mid_arr, axis_name='tp', perm=buffers)]
    all_gather x1 -> x0, waiting for transfers between devices: 48.5 us -> none  [per_device(): lax.all_gather((gain_a * gate_first).astype(jnp.bfloat16), 'tp', axis=1,...]
    all_to_all x1, waiting for transfers between devices: 95.9 us -> 134 us  [per_device(): lax.all_to_all(wide[0], 'fs', split_axis=1, concat_axis=0, tiled=True)]
    all_gather x1, waiting for transfers between devices: 30.9 us -> 0.02 us  [per_device(): lax.all_gather((gain_a * up_first).astype(jnp.bfloat16), 'tp', axis=1, ti...]
    all_gather x1, waiting for transfers between devices: 35.5 us -> 18.7 us  [per_device(): lax.all_gather(down_first.astype(jnp.bfloat16), 'tp', axis=1, tiled=True)]
    ppermute x0 -> x3, starting transfers between devices: none -> 9.11 us  [the longest x2 7.17 us: arrange_thing_over_axis(): mid_arr = lax.ppermute(mid_arr, axis_name='tp', perm=buffers)]
    unnamed x22 -> x18, local copies, waits for them, and re-layouts: 30.9 us -> 26.1 us
  transfers between devices with their start and end apart: 12 -> 14, of which waited for: 9 -> 9; matrix products, arithmetic and copies ran while one was open for 7% -> 9% of each run, Pallas kernels for 0% -> 0%
where the time goes in v1:
time: 878 us; the launch traced here: 877 us
  waiting for transfers between devices  719 us (82%)
  local copies, waits for them, and re-layouts  66.7 us (8%)
  starting transfers between devices  30.7 us (3%)
  matrix products  23.6 us (3%)
  other arithmetic  22.3 us (3%)
  between operations  14.3 us (2%)
    psum x2, waiting for transfers between devices, half_step(): total = lax.psum(partial_value, 'fs')  220 us
    all_to_all x1, waiting for transfers between devices, per_device(): lax.all_to_all(wide[0], 'fs', split_axis=1, concat_axis=0, tiled=True)  134 us
    all_to_all x1, waiting for transfers between devices, per_device(): lax.all_to_all(wide[1], 'fs', split_axis=1, concat_axis=0, tiled=True)  131 us
    all_to_all x1, waiting for transfers between devices, per_device(): lax.all_to_all(wide[3], 'fs', split_axis=1, concat_axis=0, tiled=True)  101 us
    ppermute x2, waiting for transfers between devices, arrange_thing_over_axis(): mid_arr = lax.ppermute(mid_arr, axis_name='tp', perm=buffers)  75 us
    all_gather x1, waiting for transfers between devices, per_device(): lax.all_gather(down_second.astype(jnp.bfloat16), 'tp', axis=1, tiled=True)  37.7 us
    unnamed x18, local copies, waits for them, and re-layouts  26.1 us
    all_gather x1, waiting for transfers between devices, per_device(): lax.all_gather(down_first.astype(jnp.bfloat16), 'tp', axis=1, tiled=True)  18.7 us
  transfers between devices with their start and end apart: 14, of which 9 were waited for; matrix products, arithmetic and copies ran while one was open for 9% of the time, Pallas kernels for 0%

profile of v1, /device:TPU:0, one launch (start us, length us, event | category | flops | bytes accessed | tf_op | source)
XLA Modules:
  0.0 876.7 jit_solution(7763050995130494224)
XLA Ops:
  7.2 2.4 copy.28
  9.6 0.8 dynamic_slice.6
  10.4 1.4 multiply_convert_fusion.2
  11.8 2.4 copy.26
  14.2 3.2 broadcast_in_dim.2
  17.4 2.0 constant_dynamic-update-slice_fusion.3
  19.4 0.5 collective-permute-start
  19.9 1.9 collective-permute-start.1
  21.9 61.8 %collective-permute-done = bf16[384,2048]{0,1:T(8,128)(2,1)S(1)} collective-permute-done((bf16[384,2048]{0,1:T(8,128)(2,1)}, bf16[384,2048]{0,1:T(8,128)(2,1)S(1)}, u32[]{:S(2)}, u32[]{:S(2)}) %collective-permute-start) | collective-permute-done | bytes 1572896 | tf_op jit(solution)/shard_map/ppermute | solution.py:47
  83.7 6.7 collective-permute-start.2
  90.4 1.3 constant_dynamic-update-slice_fusion.2
  91.7 2.7 constant_dynamic-update-slice_fusion.1
  94.4 13.2 %collective-permute-done.2 = bf16[384,2048]{0,1:T(8,128)(2,1)S(1)} collective-permute-done((bf16[384,2048]{0,1:T(8,128)(2,1)S(1)}, bf16[384,2048]{0,1:T(8,128)(2,1)S(1)}, u32[]{:S(2)}, u32[]{:S(2)}) %collective-permute-start.2) | collective-permute-done | bytes 1572896 | tf_op jit(solution)/shard_map/ppermute | solution.py:47
  107.6 1.3 constant_dynamic-update-slice_fusion
  108.9 6.8 all-to-all-start
  115.8 0.8 dynamic_slice.7
  116.6 4.5 multiply_convert_fusion.1
  121.1 134.3 %all-to-all-done = bf16[384,8,1024]{0,2,1:T(8,128)(2,1)} async-done(((bf16[384,8,1024]{0,2,1:T(8,128)(2,1)}), bf16[384,8,1024]{0,2,1:T(8,128)(2,1)}, u32[]{:S(2)}, u32[]{:S(2)}) %all-to-all-start) | async-done | bytes 6291488 | tf_op jit(solution)/shard_map/all_to_all | solution.py:71
  255.4 4.8 all-to-all-start.1
  260.2 0.7 all-gather.12.cloned.1.call-update
  261.0 6.5 copy.37
  267.5 131.3 %all-to-all-done.1 = bf16[384,8,1024]{0,2,1:T(8,128)(2,1)} async-done(((bf16[384,8,1024]{0,2,1:T(8,128)(2,1)}), bf16[384,8,1024]{0,2,1:T(8,128)(2,1)}, u32[]{:S(2)}, u32[]{:S(2)}) %all-to-all-start.1) | async-done | bytes 6291488 | tf_op jit(solution)/shard_map/all_to_all | solution.py:72
  398.7 4.7 all-to-all-start.2
  403.5 3.2 convert_element_type.47
  406.9 0.2 fusion
  407.1 6.5 copy.36
  413.6 8.8 %copy.27 = bf16[8,384,1024]{2,1,0:T(8,128)(2,1)} copy(bf16[8,384,1024]{1,2,0:T(8,128)(2,1)} %bitcast.1) | data formatting | bytes 12582912 | tf_op jit(solution)/shard_map/all_to_all | solution.py:71
  422.4 3.9 fusion.26
  426.3 8.6 copy.29
  434.9 18.7 %all-gather.8.cloned.1.call-done = bf16[1024,3072]{1,0:T(8,128)(2,1)} async-done(((bf16[1024,768]{1,0:T(8,128)(2,1)}), bf16[1024,3072]{1,0:T(8,128)(2,1)}) %all-gather.8.cloned.1.call-update) | async-done | bytes 6291472 | tf_op jit(solution)/shard_map/all_gather | solution.py:65
  453.7 7.7 fusion.9
  461.4 100.9 %all-to-all-done.2 = bf16[384,8,1024]{2,0,1:T(8,128)(2,1)} async-done(((bf16[384,8,1024]{2,0,1:T(8,128)(2,1)}), bf16[384,8,1024]{2,0,1:T(8,128)(2,1)}, u32[]{:S(2)}, u32[]{:S(2)}) %all-to-all-start.2) | async-done | bytes 6291488 | tf_op jit(solution)/shard_map/all_to_all | solution.py:73
  562.3 4.8 all-to-all-start.3
  567.2 3.2 convert_element_type.54
  570.4 0.2 all-reduce.5.cloned.1.call-start
  570.7 130.8 %all-reduce.3.cloned.1.call-done = f32[128,3072]{1,0:T(8,128)} async-done(((f32[128,3072]{1,0:T(8,128)}), f32[128,3072]{1,0:T(8,128)}) %all-reduce.3.cloned.1.call-update) | async-done | bytes 1572880 | tf_op jit(solution)/shard_map/psum | solution.py:18
  701.5 1.6 multiply_reduce_fusion.1
  703.1 1.9 fusion.3
  705.0 4.3 fusion.22
  709.4 37.7 %all-gather.14.cloned.1.call-done = bf16[1024,3072]{1,0:T(8,128)(2,1)} async-done(((bf16[1024,768]{1,0:T(8,128)(2,1)}), bf16[1024,3072]{1,0:T(8,128)(2,1)}) %all-gather.14.cloned.1.call-update) | async-done | bytes 6291472 | tf_op jit(solution)/shard_map/all_gather | solution.py:68
  747.1 7.7 fusion.8
  754.8 89.4 %all-reduce.5.cloned.1.call-done = f32[128,3072]{1,0:T(8,128)} async-done(((f32[128,3072]{1,0:T(8,128)}), f32[128,3072]{1,0:T(8,128)}) %all-reduce.5.cloned.1.call-update) | async-done | bytes 1572880 | tf_op jit(solution)/shard_map/psum | solution.py:18
  844.2 1.6 multiply_reduce_fusion
  845.9 2.6 fusion.5
  848.4 5.9 copy.48
  854.4 6.4 copy.49
  860.8 6.3 copy.50
  867.1 2.7 copy.51
  (34 shorter events, 0.5 us)
Async XLA Ops:
  7.2 113.9 %all-gather.6.cloned.1.call-start = ((), (), s32[]{:S(2)}) async-start(), calls=%async_computation.4 | async-start | bytes 7864320 | tf_op jit(solution)/shard_map/all_gather | solution.py:64
  19.4 64.3 %collective-permute-start = (bf16[384,2048]{0,1:T(8,128)(2,1)}, bf16[384,2048]{0,1:T(8,128)(2,1)S(1)}, u32[]{:S(2)}, u32[]{:S(2)}) collective-permute-start(bf16[384,2048]{0,1:T(8,128)(2,1)} %get-tuple-element.10), channel_id=1, source_target_pairs={{0,1},{1,2},{2,3},{3,0},{4,5},{5,6},{6,7},{7,4},{8,9},{9,10},{10,1... | collective-permute-start | bytes 4718600 | tf_op jit(solution)/shard_map/ppermute | solution.py:47
  19.9 71.8 %collective-permute-start.1 = (bf16[384,2048]{0,1:T(8,128)(2,1)}, bf16[384,2048]{0,1:T(8,128)(2,1)}, u32[]{:S(2)}, u32[]{:S(2)}) collective-permute-start(bf16[384,2048]{0,1:T(8,128)(2,1)} %get-tuple-element.10), channel_id=1, source_target_pairs={{0,3},{1,0},{2,1},{3,2},{4,7},{5,4},{6,5},{7,6},{8,11},{9,8},{10,9... | collective-permute-start | bytes 4718600 | tf_op jit(solution)/shard_map/ppermute | solution.py:52
  83.7 23.9 %collective-permute-start.2 = (bf16[384,2048]{0,1:T(8,128)(2,1)S(1)}, bf16[384,2048]{0,1:T(8,128)(2,1)S(1)}, u32[]{:S(2)}, u32[]{:S(2)}) collective-permute-start(bf16[384,2048]{0,1:T(8,128)(2,1)S(1)} %collective-permute-done), channel_id=1, source_target_pairs={{0,1},{1,2},{2,3},{3,0},{4,5},{5,6},{6,7},{7,4},{8,9},{9,10},{10,1... | collective-permute-start | bytes 4718600 | tf_op jit(solution)/shard_map/ppermute | solution.py:47
  108.9 7.7 copy-start.1
  108.9 146.5 %all-to-all-start = ((bf16[384,8,1024]{0,2,1:T(8,128)(2,1)}), bf16[384,8,1024]{0,2,1:T(8,128)(2,1)}, u32[]{:S(2)}, u32[]{:S(2)}) async-start(bf16[384,8,1024]{0,2,1:T(8,128)(2,1)} %bitcast), calls=%async_computation | async-start | bytes 12582912 | tf_op jit(solution)/shard_map/all_to_all | solution.py:71
  115.7 145.2 %all-gather.10.cloned.1.call-start = ((), (), s32[]{:S(2)}) async-start(), calls=%async_computation.7 | async-start | bytes 7864320 | tf_op jit(solution)/shard_map/all_gather | solution.py:66
  255.4 143.3 %all-to-all-start.1 = ((bf16[384,8,1024]{0,2,1:T(8,128)(2,1)}), bf16[384,8,1024]{0,2,1:T(8,128)(2,1)}, u32[]{:S(2)}, u32[]{:S(2)}) async-start(bf16[384,8,1024]{0,2,1:T(8,128)(2,1)} %bitcast.34), calls=%async_computation.1 | async-start | bytes 12582912 | tf_op jit(solution)/shard_map/all_to_all | solution.py:72
  260.2 146.9 %all-gather.12.cloned.1.call-start = ((), (), s32[]{:S(2)}) async-start(), calls=%async_computation.8 | async-start | bytes 7864320 | tf_op jit(solution)/shard_map/all_gather | solution.py:67
  398.7 163.6 %all-to-all-start.2 = ((bf16[384,8,1024]{2,0,1:T(8,128)(2,1)}), bf16[384,8,1024]{2,0,1:T(8,128)(2,1)}, u32[]{:S(2)}, u32[]{:S(2)}) async-start(bf16[384,8,1024]{2,0,1:T(8,128)(2,1)} %bitcast.31), calls=%async_computation.2 | async-start | bytes 12582912 | tf_op jit(solution)/shard_map/all_to_all | solution.py:73
  403.5 3.4 copy-start
  403.5 50.2 %all-gather.8.cloned.1.call-start = ((), (), s32[]{:S(2)}) async-start(), calls=%async_computation.5 | async-start | bytes 7864320 | tf_op jit(solution)/shard_map/all_gather | solution.py:65
  406.8 294.7 %all-reduce.3.cloned.1.call-start = ((), (), s32[]{:S(2)}) async-start(), calls=%async_computation.6 | async-start | bytes 3145728 | tf_op jit(solution)/shard_map/psum | solution.py:18
  562.3 184.8 %all-to-all-start.3 = ((bf16[384,8,1024]{2,0,1:T(8,128)(2,1)}), bf16[384,8,1024]{2,0,1:T(8,128)(2,1)}, u32[]{:S(2)}, u32[]{:S(2)}) async-start(bf16[384,8,1024]{2,0,1:T(8,128)(2,1)} %bitcast.28), calls=%async_computation.3 | async-start | bytes 12582912 | tf_op jit(solution)/shard_map/all_to_all | solution.py:74
  567.1 136.0 %copy-start.2 = (f32[3072]{0:T(1024)S(1)}, f32[3072]{0:T(1024)}, u32[]{:S(2)}) copy-start(f32[3072]{0:T(1024)} %param.19) | copy-start | bytes 36868
  567.1 180.0 %all-gather.14.cloned.1.call-start = ((), (), s32[]{:S(2)}) async-start(), calls=%async_computation.9 | async-start | bytes 7864320 | tf_op jit(solution)/shard_map/all_gather | solution.py:68
  570.4 273.8 %all-reduce.5.cloned.1.call-start = ((), (), s32[]{:S(2)}) async-start(), calls=%async_computation.10 | async-start | bytes 3145728 | tf_op jit(solution)/shard_map/psum | solution.py:18
  754.8 91.1 %copy-start.3 = (f32[3072]{0:T(1024)S(1)}, f32[3072]{0:T(1024)}, u32[]{:S(2)}) copy-start(f32[3072]{0:T(1024)} %param.21) | copy-start | bytes 36868
  854.4 12.7 %slice-start = ((s8[6291456]{0:T(1024)(128)(4,1)}), s8[4194304]{0:T(1024)(128)(4,1)S(1)}, s32[]{:S(2)}) async-start(s8[6291456]{0:T(1024)(128)(4,1)} %bitcast.29), calls=%async_computation.11 | async-start | bytes 8388608
  860.8 6.4 slice-start.1
Sparse Core Ops, SparseCore 0:
  11.9 81.9 all-gather.5
  121.2 49.6 all-gather.9
  263.1 46.7 all-gather.11
  406.9 46.6 all-gather.7
  461.5 239.9 all-reduce.2
  703.5 43.5 all-gather.13
  754.9 89.2 all-reduce.4
